TPU v7x, 256 devices: a 4x2x16 block of a 4x16x16 slice. The times are simulated.
256 devices in a mesh: grp: 2 (over y), sp: 32 (over z, core), tp: 4 (over x).
Axes of the slice: x: 4, y: 2, z: 16, core: 2. Of those that a mesh axis runs over, the one named last changes fastest.
The devices are a block of a 4x16x16 slice.
Arguments:
- stream: bfloat16 [16384, 4096], P(('grp', 'sp'), 'tp'), parts along dimension 0, may hold values from -6 to 6
- gain_pre: float32 [3, 4096], replicated, may hold values from 0.1 to 1.9
- w_in: bfloat16 [3, 4096, 1024], P(None, 'sp', 'tp'), may hold values from -0.09375 to 0.09375
- w_pool: bfloat16 [3, 4, 256, 256], P(None, 'tp'), may hold values from -0.375 to 0.375
- pool_scale: float32 [3, 1024], P(None, 'tp'), may hold values from 0.1 to 1.9
- w_out: bfloat16 [3, 1024, 4096], P(None, 'tp', 'sp'), may hold values from -0.5 to 0.5
- gain_post: float32 [3, 4096], replicated, may hold values from 0.1 to 1.9
Outputs:
- result: bfloat16 [16384, 4096], P(('grp', 'sp'), 'tp'), parts along dimension 0
There are 2 independent parts, one for each index of `grp`. A program takes and returns all parts, laid end to end along the dimension named above; an argument that names none is the same for every part. Nothing has to cross between parts.
All inputs are finite; a program needn't handle non-finite values.
Results may differ from a plain program's by a relative error of at most 0.02.
Values may be sent and summed in bfloat16 or wider, within the bound.
A program may use at most 64 MiB of HBM per device.

v0:
```python
import jax
import jax.numpy as jnp
from jax import lax
from jax.sharding import PartitionSpec as P

LAYERS = 3
WINDOWS = (2, 4, 8, 16)
EPS = 1e-06


def rows_first(arrays, axis, dims):
    turned = [jnp.moveaxis(a, dim, 0) for a, dim in zip(arrays, dims)]
    widths = [t[0].size for t in turned]
    both = jnp.concatenate([t.reshape(-1, w) for t, w in zip(turned, widths)], axis=1)
    result = lax.all_gather(both, axis, axis=0, tiled=True)
    tiles = jnp.split(result, [sum(widths[:k]) for k in range(1, len(widths))], axis=1)
    return tuple(
        (
            jnp.moveaxis(b.reshape(-1, *t.shape[1:]), 0, dim)
            for b, t, dim in zip(tiles, turned, dims)
        )
    )


def from_behind(block, axis, distance):
    devices = range(lax.axis_size(axis))
    route = [(i - distance, i) for i in devices if i - distance in devices]
    return lax.ppermute(block, axis, route)


def copy_for_each(array, axis):
    copies = jnp.broadcast_to(array, (lax.axis_size(axis), *array.shape))
    return lax.all_to_all(copies, axis, split_axis=0, concat_axis=0, tiled=True)


def joined_along(tiles, dim):
    tiles = jnp.moveaxis(tiles, 0, dim)
    dims = tiles.shape
    return tiles.reshape(*dims[:dim], dims[dim] * dims[dim + 1], *dims[dim + 2 :])


def gather_directly(array, axis, dim):
    tiles = copy_for_each(array, axis)
    return joined_along(tiles, dim)


def in_blocks(array, dim, size):
    before, after = (array.shape[:dim], array.shape[dim + 1 :])
    return jnp.moveaxis(array.reshape(*before, size, -1, *after), dim, 0)


def sent_and_summed(array, axis, dim):
    size = lax.axis_size(axis)
    tiles = lax.all_to_all(in_blocks(array, dim, size), axis, 0, 0, tiled=True)
    return jnp.sum(tiles.astype(jnp.float32), axis=0)


def taken_together(array, axis):
    everything = copy_for_each(array, axis)
    return jnp.sum(everything, axis=0)


def rms_scale(values, gain):
    inverse = lax.rsqrt(jnp.mean(values * values, axis=-1, keepdims=True) + EPS)
    return values * inverse * gain[None, :]


def per_device(stream, gain_pre, w_in, w_pool, pool_scale, w_out, gain_post):
    tok_rows = stream.shape[0]
    block_width = stream.shape[1]
    width = gain_pre.shape[1]
    group = w_pool.shape[2]
    reach = max(WINDOWS) - 1
    group_index = lax.axis_index("tp")
    window = jnp.where(
        group_index == 0, 2, jnp.where(group_index == 1, 4, jnp.where(group_index == 2, 8, 16))
    )
    positions = lax.axis_index("sp") * tok_rows + lax.iota(jnp.int32, tok_rows)
    count = jnp.minimum(positions + 1, window).astype(jnp.float32)
    gathered_in, gathered_out = rows_first((w_in, w_out), "sp", (1, 2))
    current = stream
    feature_start = group_index * block_width
    for layer in range(LAYERS):
        full_rows = gather_directly(current, "tp", 1)
        normed = rms_scale(full_rows.astype(jnp.float32), gain_pre[layer]).astype(jnp.bfloat16)
        inner_sum = jnp.dot(normed, gathered_in[layer], preferred_element_type=jnp.float32)
        inner = inner_sum.astype(jnp.bfloat16)
        rim = from_behind(inner[tok_rows - reach :], "sp", 1)
        extended = jnp.concatenate([rim, inner], axis=0).astype(jnp.float32)
        summed = jnp.zeros((tok_rows, group), jnp.float32)
        for offset in range(max(WINDOWS)):
            window_slice = extended[reach - offset : reach - offset + tok_rows]
            summed = summed + jnp.where(offset < window, window_slice, 0.0)
        pooled = summed / count[:, None]
        spread = (pooled - inner.astype(jnp.float32)).astype(jnp.bfloat16)
        mixed = jnp.dot(spread, w_pool[layer, 0], preferred_element_type=jnp.float32)
        mixed = (mixed * pool_scale[layer][None, :]).astype(jnp.bfloat16)
        partial_value = jnp.dot(mixed, gathered_out[layer], preferred_element_type=jnp.float32)
        partial_value = partial_value.astype(jnp.bfloat16)
        branch = sent_and_summed(partial_value, "tp", 1)
        squares = taken_together(jnp.sum(branch * branch, axis=1), "tp")
        inverse = lax.rsqrt(squares / width + EPS)
        gain_block = lax.dynamic_slice_in_dim(gain_post[layer], feature_start, block_width, 0)
        normed_branch = branch * inverse[:, None] * gain_block[None, :]
        current = (current.astype(jnp.float32) + normed_branch).astype(jnp.bfloat16)
    return current


def solution(mesh):
    return jax.shard_map(
        per_device,
        mesh=mesh,
        in_specs=(
            P(("grp", "sp"), "tp"),
            P(),
            P(None, "sp", "tp"),
            P(None, "tp", None, None),
            P(None, "tp"),
            P(None, "tp", "sp"),
            P(),
        ),
        out_specs=P(("grp", "sp"), "tp"),
        check_vma=False,
    )
```

profile of v0, /device:TPU:33, one launch (start us, length us, event | category | flops | bytes accessed | tf_op | source)
XLA Modules:
  0.0 364.8 jit_solution(6693995348859287650)
XLA Ops:
  6.5 0.0 all-gather.2.cloned.1.call-start
  6.6 1.1 copy.27
  7.6 1.7 pad_maximum_fusion
  9.3 0.1 all-gather.2.cloned.1.call-update
  9.4 1.2 copy.26
  10.7 1.5 broadcast_in_dim.81
  12.2 5.2 %all-to-all-start = ((bf16[4,256,1024]{1,2,0:T(8,128)(2,1)}), bf16[4,256,1024]{1,2,0:T(8,128)(2,1)S(1)}, u32[]{:S(2)}, u32[]{:S(2)}) async-start(bf16[4,256,1024]{1,2,0:T(8,128)(2,1)} %broadcast_in_dim.81), calls=%async_computation | async-start | bytes 4194304 | tf_op jit(solution)/shard_map/all_to_all | solution.py:33
  17.4 0.1 slice_reduce_fusion
  17.6 15.2 %all-to-all-done = bf16[4,256,1024]{1,2,0:T(8,128)(2,1)S(1)} async-done(((bf16[4,256,1024]{1,2,0:T(8,128)(2,1)}), bf16[4,256,1024]{1,2,0:T(8,128)(2,1)S(1)}, u32[]{:S(2)}, u32[]{:S(2)}) %all-to-all-start) | async-done | bytes 2097184 | tf_op jit(solution)/shard_map/all_to_all | solution.py:33
  32.8 0.6 fusion
  33.3 1.7 fusion.2
  35.0 101.4 %all-gather.2.cloned.1.call-done = bf16[4096,1536]{0,1:T(8,128)(2,1)} async-done(((bf16[128,1536]{0,1:T(8,128)(2,1)}), bf16[4096,1536]{0,1:T(8,128)(2,1)}) %all-gather.2.cloned.1.call-update) | async-done | bytes 12582928 | tf_op jit(solution)/shard_map/all_gather | solution.py:15
  136.4 8.4 %fusion.207 = (bf16[4096,768]{0,1:T(8,128)(2,1)S(1)}, bf16[4096,768]{0,1:T(8,128)(2,1)}) fusion(bf16[4096,1536]{0,1:T(8,128)(2,1)} %all-gather.2.cloned.1.call-done), kind=kLoop, calls=%fused_computation.233 | loop fusion | bytes 25165824 | tf_op jit(solution)/shard_map/split | solution.py:16
  144.8 2.7 copy-done
  147.5 0.0 copy-done.1
  147.5 0.8 fusion.15
  148.3 4.7 %collective-permute-start = (bf16[15,256]{1,0:T(8,128)(2,1)S(1)}, bf16[15,256]{1,0:T(8,128)(2,1)S(1)}, u32[]{:S(2)}, u32[]{:S(2)}) collective-permute-start(bf16[15,256]{1,0:T(8,128)(2,1)S(1)} %slice.277), channel_id=1, source_target_pairs={{0,4},{4,8},{8,12},{12,16},{16,20},{20,24},{24,28},{28,32},{32,36}... | collective-permute-start | bytes 23048 | tf_op jit(solution)/shard_map/ppermute | solution.py:28
  153.0 0.7 collective-permute-done
  153.8 3.0 convolution_convert_fusion.2
  156.8 1.6 copy.47
  158.4 4.1 %all-to-all-start.1 = ((bf16[4,256,1024]{2,1,0:T(8,128)(2,1)}), bf16[4,256,1024]{2,1,0:T(8,128)(2,1)S(1)}, u32[]{:S(2)}, u32[]{:S(2)}) async-start(bf16[4,256,1024]{2,1,0:T(8,128)(2,1)} %bitcast.87), calls=%async_computation.1 | async-start | bytes 4194304 | tf_op jit(solution)/shard_map/all_to_all | solution.py:54
  162.5 25.9 %all-to-all-done.1 = bf16[4,256,1024]{2,1,0:T(8,128)(2,1)S(1)} async-done(((bf16[4,256,1024]{2,1,0:T(8,128)(2,1)}), bf16[4,256,1024]{2,1,0:T(8,128)(2,1)S(1)}, u32[]{:S(2)}, u32[]{:S(2)}) %all-to-all-start.1) | async-done | bytes 2097184 | tf_op jit(solution)/shard_map/all_to_all | solution.py:54
  188.5 0.4 convert_reduce_fusion.2
  188.8 0.1 multiply_reduce_fusion.2
  189.0 0.6 broadcast_in_dim.83
  189.6 3.3 all-to-all-start.2
  193.0 4.0 %all-to-all-done.2 = f32[4,1,256]{2,1,0:T(1,128)S(1)} async-done(((f32[4,1,256]{2,1,0:T(1,128)}), f32[4,1,256]{2,1,0:T(1,128)S(1)}, u32[]{:S(2)}, u32[]{:S(2)}) %all-to-all-start.2) | async-done | bytes 4128 | tf_op jit(solution)/shard_map/all_to_all | solution.py:33
  197.0 1.3 add_convert_fusion.2
  198.3 0.2 copy.30
  198.5 1.5 broadcast_in_dim.84
  200.0 3.7 %all-to-all-start.3 = ((bf16[4,256,1024]{1,2,0:T(8,128)(2,1)}), bf16[4,256,1024]{1,2,0:T(8,128)(2,1)S(1)}, u32[]{:S(2)}, u32[]{:S(2)}) async-start(bf16[4,256,1024]{1,2,0:T(8,128)(2,1)} %broadcast_in_dim.84), calls=%async_computation.3 | async-start | bytes 4194304 | tf_op jit(solution)/shard_map/all_to_all | solution.py:33
  203.7 23.8 %all-to-all-done.3 = bf16[4,256,1024]{1,2,0:T(8,128)(2,1)S(1)} async-done(((bf16[4,256,1024]{1,2,0:T(8,128)(2,1)}), bf16[4,256,1024]{1,2,0:T(8,128)(2,1)S(1)}, u32[]{:S(2)}, u32[]{:S(2)}) %all-to-all-start.3) | async-done | bytes 2097184 | tf_op jit(solution)/shard_map/all_to_all | solution.py:33
  227.6 0.6 fusion.3
  228.1 0.7 fusion.5
  228.9 2.4 fusion.16
  231.3 3.0 collective-permute-start.1
  234.3 2.3 collective-permute-done.1
  236.6 3.0 convolution_convert_fusion.1
  239.6 0.2 copy.46
  239.8 28.6 %all_to_all.48 = bf16[4,256,1024]{2,1,0:T(8,128)(2,1)S(1)} all-to-all(bf16[4,256,1024]{2,1,0:T(8,128)(2,1)S(1)} %bitcast.88), channel_id=1, replica_groups=mesh['grp'=2,'sp'=32,'tp'=4] {'tp'}, dimensions={0} | all-to-all | bytes 4194304 | tf_op jit(solution)/shard_map/all_to_all | solution.py:54
  268.4 0.4 convert_reduce_fusion.1
  268.8 0.1 multiply_reduce_fusion.1
  268.9 0.6 broadcast_in_dim.85
  269.5 3.3 all-to-all-start.5
  272.9 4.0 %all-to-all-done.5 = f32[4,1,256]{2,1,0:T(1,128)S(1)} async-done(((f32[4,1,256]{2,1,0:T(1,128)}), f32[4,1,256]{2,1,0:T(1,128)S(1)}, u32[]{:S(2)}, u32[]{:S(2)}) %all-to-all-start.5) | async-done | bytes 4128 | tf_op jit(solution)/shard_map/all_to_all | solution.py:33
  277.0 0.2 add_convert_fusion.1
  277.2 0.2 copy.33
  277.4 1.5 broadcast_in_dim.86
  278.9 3.9 %all-to-all-start.6 = ((bf16[4,256,1024]{1,2,0:T(8,128)(2,1)}), bf16[4,256,1024]{1,2,0:T(8,128)(2,1)S(1)}, u32[]{:S(2)}, u32[]{:S(2)}) async-start(bf16[4,256,1024]{1,2,0:T(8,128)(2,1)} %broadcast_in_dim.86), calls=%async_computation.6 | async-start | bytes 4194304 | tf_op jit(solution)/shard_map/all_to_all | solution.py:33
  282.8 23.8 %all-to-all-done.6 = bf16[4,256,1024]{1,2,0:T(8,128)(2,1)S(1)} async-done(((bf16[4,256,1024]{1,2,0:T(8,128)(2,1)}), bf16[4,256,1024]{1,2,0:T(8,128)(2,1)S(1)}, u32[]{:S(2)}, u32[]{:S(2)}) %all-to-all-start.6) | async-done | bytes 2097184 | tf_op jit(solution)/shard_map/all_to_all | solution.py:33
  306.6 0.6 fusion.6
  307.2 0.7 fusion.8
  307.9 2.4 fusion.17
  310.3 6.9 %collective-permute-start.2 = (bf16[15,256]{1,0:T(8,128)(2,1)S(1)}, bf16[15,256]{1,0:T(8,128)(2,1)S(1)}, u32[]{:S(2)}, u32[]{:S(2)}) collective-permute-start(bf16[15,256]{1,0:T(8,128)(2,1)S(1)} %slice.315), channel_id=1, source_target_pairs={{0,4},{4,8},{8,12},{12,16},{16,20},{20,24},{24,28},{28,32},{32,36}... | collective-permute-start | bytes 23048 | tf_op jit(solution)/shard_map/ppermute | solution.py:28
  317.2 0.8 collective-permute-done.2
  318.0 3.0 convolution_convert_fusion
  321.0 0.2 copy.45
  321.2 27.2 %all_to_all.49 = bf16[4,256,1024]{2,1,0:T(8,128)(2,1)S(1)} all-to-all(bf16[4,256,1024]{2,1,0:T(8,128)(2,1)S(1)} %bitcast.89), channel_id=1, replica_groups=mesh['grp'=2,'sp'=32,'tp'=4] {'tp'}, dimensions={0} | all-to-all | bytes 4194304 | tf_op jit(solution)/shard_map/all_to_all | solution.py:54
  348.4 0.4 convert_reduce_fusion
  348.8 0.1 multiply_reduce_fusion
  348.9 0.6 broadcast_in_dim.87
  349.5 3.3 all-to-all-start.8
  352.9 4.0 %all-to-all-done.8 = f32[4,1,256]{2,1,0:T(1,128)S(1)} async-done(((f32[4,1,256]{2,1,0:T(1,128)}), f32[4,1,256]{2,1,0:T(1,128)S(1)}, u32[]{:S(2)}, u32[]{:S(2)}) %all-to-all-start.8) | async-done | bytes 4128 | tf_op jit(solution)/shard_map/all_to_all | solution.py:33
  356.9 1.0 add_convert_fusion
  (32 shorter events, 0.4 us)
Async XLA Ops:
  6.5 129.9 %all-gather.2.cloned.1.call-start = ((), (), s32[]{:S(2)}) async-start(), calls=%async_computation.9 | async-start | bytes 12976128 | tf_op jit(solution)/shard_map/all_gather | solution.py:15
  12.2 5.3 %copy-start.2 = (f32[3,4096]{1,0:T(4,128)S(1)}, f32[3,4096]{1,0:T(4,128)}, u32[]{:S(2)}) copy-start(f32[3,4096]{1,0:T(4,128)} %param.8) | copy-start | bytes 147460
  12.2 5.4 %copy-start.4 = (f32[3,256]{1,0:T(4,128)S(1)}, f32[3,256]{1,0:T(4,128)}, u32[]{:S(2)}) copy-start(f32[3,256]{1,0:T(4,128)} %param.11) | copy-start | bytes 9220
  12.2 20.6 %all-to-all-start = ((bf16[4,256,1024]{1,2,0:T(8,128)(2,1)}), bf16[4,256,1024]{1,2,0:T(8,128)(2,1)S(1)}, u32[]{:S(2)}, u32[]{:S(2)}) async-start(bf16[4,256,1024]{1,2,0:T(8,128)(2,1)} %broadcast_in_dim.81), calls=%async_computation | async-start | bytes 4194304 | tf_op jit(solution)/shard_map/all_to_all | solution.py:33
  35.0 112.5 %copy-start.1 = (bf16[4,256,1024]{1,2,0:T(8,128)(2,1)S(1)}, bf16[4,256,1024]{1,2,0:T(8,128)(2,1)}, u32[]{:S(2)}) copy-start(bf16[4,256,1024]{1,2,0:T(8,128)(2,1)} %fusion.2) | copy-start | bytes 6291460
  144.8 2.7 copy-start
  148.3 5.4 %collective-permute-start = (bf16[15,256]{1,0:T(8,128)(2,1)S(1)}, bf16[15,256]{1,0:T(8,128)(2,1)S(1)}, u32[]{:S(2)}, u32[]{:S(2)}) collective-permute-start(bf16[15,256]{1,0:T(8,128)(2,1)S(1)} %slice.277), channel_id=1, source_target_pairs={{0,4},{4,8},{8,12},{12,16},{16,20},{20,24},{24,28},{28,32},{32,36}... | collective-permute-start | bytes 23048 | tf_op jit(solution)/shard_map/ppermute | solution.py:28
  158.4 4.1 %copy-start.3 = (f32[3,4096]{1,0:T(4,128)S(1)}, f32[3,4096]{1,0:T(4,128)}, u32[]{:S(2)}) copy-start(f32[3,4096]{1,0:T(4,128)} %param.13) | copy-start | bytes 147460
  158.4 30.1 %all-to-all-start.1 = ((bf16[4,256,1024]{2,1,0:T(8,128)(2,1)}), bf16[4,256,1024]{2,1,0:T(8,128)(2,1)S(1)}, u32[]{:S(2)}, u32[]{:S(2)}) async-start(bf16[4,256,1024]{2,1,0:T(8,128)(2,1)} %bitcast.87), calls=%async_computation.1 | async-start | bytes 4194304 | tf_op jit(solution)/shard_map/all_to_all | solution.py:54
  189.6 7.4 %all-to-all-start.2 = ((f32[4,1,256]{2,1,0:T(1,128)}), f32[4,1,256]{2,1,0:T(1,128)S(1)}, u32[]{:S(2)}, u32[]{:S(2)}) async-start(f32[4,1,256]{2,1,0:T(1,128)} %broadcast_in_dim.83), calls=%async_computation.2 | async-start | bytes 8192 | tf_op jit(solution)/shard_map/all_to_all | solution.py:33
  200.0 27.6 %all-to-all-start.3 = ((bf16[4,256,1024]{1,2,0:T(8,128)(2,1)}), bf16[4,256,1024]{1,2,0:T(8,128)(2,1)S(1)}, u32[]{:S(2)}, u32[]{:S(2)}) async-start(bf16[4,256,1024]{1,2,0:T(8,128)(2,1)} %broadcast_in_dim.84), calls=%async_computation.3 | async-start | bytes 4194304 | tf_op jit(solution)/shard_map/all_to_all | solution.py:33
  231.3 5.3 %collective-permute-start.1 = (bf16[15,256]{1,0:T(8,128)(2,1)S(1)}, bf16[15,256]{1,0:T(8,128)(2,1)S(1)}, u32[]{:S(2)}, u32[]{:S(2)}) collective-permute-start(bf16[15,256]{1,0:T(8,128)(2,1)S(1)} %slice.296), channel_id=1, source_target_pairs={{0,4},{4,8},{8,12},{12,16},{16,20},{20,24},{24,28},{28,32},{32,36}... | collective-permute-start | bytes 23048 | tf_op jit(solution)/shard_map/ppermute | solution.py:28
  269.5 7.4 %all-to-all-start.5 = ((f32[4,1,256]{2,1,0:T(1,128)}), f32[4,1,256]{2,1,0:T(1,128)S(1)}, u32[]{:S(2)}, u32[]{:S(2)}) async-start(f32[4,1,256]{2,1,0:T(1,128)} %broadcast_in_dim.85), calls=%async_computation.5 | async-start | bytes 8192 | tf_op jit(solution)/shard_map/all_to_all | solution.py:33
  278.9 27.7 %all-to-all-start.6 = ((bf16[4,256,1024]{1,2,0:T(8,128)(2,1)}), bf16[4,256,1024]{1,2,0:T(8,128)(2,1)S(1)}, u32[]{:S(2)}, u32[]{:S(2)}) async-start(bf16[4,256,1024]{1,2,0:T(8,128)(2,1)} %broadcast_in_dim.86), calls=%async_computation.6 | async-start | bytes 4194304 | tf_op jit(solution)/shard_map/all_to_all | solution.py:33
  310.3 7.7 %collective-permute-start.2 = (bf16[15,256]{1,0:T(8,128)(2,1)S(1)}, bf16[15,256]{1,0:T(8,128)(2,1)S(1)}, u32[]{:S(2)}, u32[]{:S(2)}) collective-permute-start(bf16[15,256]{1,0:T(8,128)(2,1)S(1)} %slice.315), channel_id=1, source_target_pairs={{0,4},{4,8},{8,12},{12,16},{16,20},{20,24},{24,28},{28,32},{32,36}... | collective-permute-start | bytes 23048 | tf_op jit(solution)/shard_map/ppermute | solution.py:28
  349.5 7.4 %all-to-all-start.8 = ((f32[4,1,256]{2,1,0:T(1,128)}), f32[4,1,256]{2,1,0:T(1,128)S(1)}, u32[]{:S(2)}, u32[]{:S(2)}) async-start(f32[4,1,256]{2,1,0:T(1,128)} %broadcast_in_dim.87), calls=%async_computation.8 | async-start | bytes 8192 | tf_op jit(solution)/shard_map/all_to_all | solution.py:33
Sparse Core Ops, SparseCore 0:
  9.5 126.8 all-gather.1
where the time goes:
time: 366 us; the launch traced here: 365 us
  waiting for transfers between devices  206 us (56%)
  blocking collectives  55.8 us (15%)
  starting transfers between devices  41.5 us (11%)
  local copies, waits for them, and re-layouts  22.3 us (6%)
  matrix products  14.6 us (4%)
  between operations  13.8 us (4%)
  other arithmetic  10.9 us (3%)
    all_gather x1, waiting for transfers between devices, rows_first(): result = lax.all_gather(both, axis, axis=0, tiled=True)  101 us
    all_to_all x6, waiting for transfers between devices, copy_for_each(): return lax.all_to_all(copies, axis, split_axis=0, concat_axis=0, tiled=True)  74.9 us
    all_to_all x2, blocking collectives, sent_and_summed(): tiles = lax.all_to_all(in_blocks(array, dim, size), axis, 0, 0, tiled=True)  55.8 us
    all_to_all x1, waiting for transfers between devices, sent_and_summed(): tiles = lax.all_to_all(in_blocks(array, dim, size), axis, 0, 0, tiled=True)  25.9 us
    all_to_all x6, starting transfers between devices, copy_for_each(): return lax.all_to_all(copies, axis, split_axis=0, concat_axis=0, tiled=True)  22.8 us
    ppermute x3, starting transfers between devices, from_behind(): return lax.ppermute(block, axis, route)  14.5 us
    dot_general x3, matrix products, per_device(): jnp.dot(mixed, gathered_out[layer], preferred_element_type=jnp.float32)  9.05 us
    split x1, local copies, waits for them, and re-layouts, rows_first(): jnp.split(result, [sum(widths[:k]) for k in range(1, len(widths))], axis=1)  8.43 us
  transfers between devices with their start and end apart: 11, of which 11 were waited for; matrix products, arithmetic and copies ran while one was open for 1% of the time, Pallas kernels for 0%

commit v1 on v0

--- a/solution.py
+++ b/solution.py
@@ -12,7 +12,8 @@
     turned = [jnp.moveaxis(a, dim, 0) for a, dim in zip(arrays, dims)]
     widths = [t[0].size for t in turned]
     both = jnp.concatenate([t.reshape(-1, w) for t, w in zip(turned, widths)], axis=1)
-    result = lax.all_gather(both, axis, axis=0, tiled=True)
+    stack = jnp.stack([both] * lax.axis_size(axis))
+    result = jnp.concatenate(lax.all_to_all(stack, axis, 0, 0), axis=0)
     tiles = jnp.split(result, [sum(widths[:k]) for k in range(1, len(widths))], axis=1)
     return tuple(
         (

time: 366 us -> 834 us (2.28); the launches traced: 365 us -> 824 us
  waiting for transfers between devices: 206 us -> 612 us
  starting transfers between devices: 41.5 us -> 121 us
  blocking collectives: 55.8 us -> 35.8 us
  between operations: 13.8 us -> 0.42 us
    all_to_all x0 -> x1, waiting for transfers between devices: none -> 535 us  [rows_first(): result = jnp.concatenate(lax.all_to_all(stack, axis, 0, 0), axis=0)]
    all_gather x1 -> x0, waiting for transfers between devices: 101 us -> none  [rows_first(): result = lax.all_gather(both, axis, axis=0, tiled=True)]
    ppermute x3, starting transfers between devices: 14.5 us -> 54.5 us  [from_behind(): return lax.ppermute(block, axis, route)]
    all_to_all x0 -> x1, starting transfers between devices: none -> 36.1 us  [rows_first(): result = jnp.concatenate(lax.all_to_all(stack, axis, 0, 0), axis=0)]
    all_to_all x2, blocking collectives: 55.8 us -> 35.8 us  [sent_and_summed(): tiles = lax.all_to_all(in_blocks(array, dim, size), axis, 0, 0, tiled=True)]
    all_to_all x6, waiting for transfers between devices: 74.9 us -> 59.8 us  [copy_for_each(): return lax.all_to_all(copies, axis, split_axis=0, concat_axis=0, tiled=True)]
    all_to_all x1, waiting for transfers between devices: 25.9 us -> 15.2 us  [sent_and_summed(): tiles = lax.all_to_all(in_blocks(array, dim, size), axis, 0, 0, tiled=True)]
  transfers between devices with their start and end apart: 11 -> 11, of which waited for: 11 -> 11; matrix products, arithmetic and copies ran while one was open for 1% -> 0% of each run, Pallas kernels for 0% -> 0%
where the time goes in v1:
time: 834 us; the launch traced here: 824 us
  waiting for transfers between devices  612 us (73%)
  starting transfers between devices  121 us (15%)
  blocking collectives  35.8 us (4%)
  local copies, waits for them, and re-layouts  30.6 us (4%)
  matrix products  14.5 us (2%)
  other arithmetic  9.25 us (1%)
    all_to_all x1, waiting for transfers between devices, rows_first(): result = jnp.concatenate(lax.all_to_all(stack, axis, 0, 0), axis=0)  535 us
    all_to_all x6, waiting for transfers between devices, copy_for_each(): return lax.all_to_all(copies, axis, split_axis=0, concat_axis=0, tiled=True)  59.8 us
    ppermute x3, starting transfers between devices, from_behind(): return lax.ppermute(block, axis, route)  54.5 us
    all_to_all x1, starting transfers between devices, rows_first(): result = jnp.concatenate(lax.all_to_all(stack, axis, 0, 0), axis=0)  36.1 us
    all_to_all x2, blocking collectives, sent_and_summed(): tiles = lax.all_to_all(in_blocks(array, dim, size), axis, 0, 0, tiled=True)  35.8 us
    all_to_all x6, starting transfers between devices, copy_for_each(): return lax.all_to_all(copies, axis, split_axis=0, concat_axis=0, tiled=True)  26.2 us
  transfers between devices with their start and end apart: 11, of which 11 were waited for; matrix products, arithmetic and copies ran while one was open for 0% of the time, Pallas kernels for 0%

profile of v1, /device:TPU:33, one launch (start us, length us, event | category | flops | bytes accessed | tf_op | source)
XLA Modules:
  0.0 823.5 jit_solution(4230152748036874111)
XLA Ops:
  0.0 1.2 copy.38
  1.2 1.5 broadcast_in_dim.81
  2.7 5.2 all-to-all-start
  8.0 0.2 copy.39
  8.2 15.1 %all-to-all-done = bf16[4,256,1024]{1,2,0:T(8,128)(2,1)S(1)} async-done(((bf16[4,256,1024]{1,2,0:T(8,128)(2,1)}), bf16[4,256,1024]{1,2,0:T(8,128)(2,1)S(1)}, u32[]{:S(2)}, u32[]{:S(2)}) %all-to-all-start) | async-done | bytes 2097184 | tf_op jit(solution)/shard_map/all_to_all | solution.py:34
  23.3 7.3 stack.2
  30.7 36.1 %all-to-all-start.1 = ((bf16[32,128,1536]{1,2,0:T(8,128)(2,1)}), bf16[32,128,1536]{1,2,0:T(8,128)(2,1)}, u32[]{:S(2)}, u32[]{:S(2)}) async-start(bf16[32,128,1536]{1,2,0:T(8,128)(2,1)} %stack.2), calls=%async_computation.1 | async-start | bytes 25165824 | tf_op jit(solution)/shard_map/all_to_all | solution.py:16
  66.8 0.0 copy-done.4
  66.8 0.1 slice_reduce_fusion
  67.0 0.6 fusion
  67.6 1.7 fusion.2
  69.3 535.2 %all-to-all-done.1 = bf16[32,128,1536]{1,2,0:T(8,128)(2,1)} async-done(((bf16[32,128,1536]{1,2,0:T(8,128)(2,1)}), bf16[32,128,1536]{1,2,0:T(8,128)(2,1)}, u32[]{:S(2)}, u32[]{:S(2)}) %all-to-all-start.1) | async-done | bytes 12582944 | tf_op jit(solution)/shard_map/all_to_all | solution.py:16
  604.5 6.7 copy_bitcast_fusion
  611.2 3.7 fusion.207
  614.9 2.7 copy-done
  617.6 0.8 fusion.15
  618.4 15.1 %collective-permute-start = (bf16[15,256]{1,0:T(8,128)(2,1)S(1)}, bf16[15,256]{1,0:T(8,128)(2,1)S(1)}, u32[]{:S(2)}, u32[]{:S(2)}) collective-permute-start(bf16[15,256]{1,0:T(8,128)(2,1)S(1)} %slice.277), channel_id=1, source_target_pairs={{0,4},{4,8},{8,12},{12,16},{16,20},{20,24},{24,28},{28,32},{32,36}... | collective-permute-start | bytes 23048 | tf_op jit(solution)/shard_map/ppermute | solution.py:29
  633.5 0.7 collective-permute-done
  634.2 3.0 convolution_convert_fusion.2
  637.3 1.6 copy.65
  638.8 3.8 all-to-all-start.2
  642.7 15.2 %all-to-all-done.2 = bf16[4,256,1024]{2,1,0:T(8,128)(2,1)S(1)} async-done(((bf16[4,256,1024]{2,1,0:T(8,128)(2,1)}), bf16[4,256,1024]{2,1,0:T(8,128)(2,1)S(1)}, u32[]{:S(2)}, u32[]{:S(2)}) %all-to-all-start.2) | async-done | bytes 2097184 | tf_op jit(solution)/shard_map/all_to_all | solution.py:55
  658.0 0.4 convert_reduce_fusion.2
  658.3 0.1 multiply_reduce_fusion.2
  658.5 0.6 broadcast_in_dim.83
  659.1 3.3 all-to-all-start.3
  662.5 4.0 all-to-all-done.3
  666.5 1.3 add_convert_fusion.2
  667.8 0.2 copy.44
  668.0 1.5 broadcast_in_dim.84
  669.5 3.7 all-to-all-start.4
  673.2 17.2 %all-to-all-done.4 = bf16[4,256,1024]{1,2,0:T(8,128)(2,1)S(1)} async-done(((bf16[4,256,1024]{1,2,0:T(8,128)(2,1)}), bf16[4,256,1024]{1,2,0:T(8,128)(2,1)S(1)}, u32[]{:S(2)}, u32[]{:S(2)}) %all-to-all-start.4) | async-done | bytes 2097184 | tf_op jit(solution)/shard_map/all_to_all | solution.py:34
  690.4 0.6 fusion.3
  691.0 0.7 fusion.5
  691.7 2.4 fusion.16
  694.1 20.6 %collective-permute-start.1 = (bf16[15,256]{1,0:T(8,128)(2,1)S(1)}, bf16[15,256]{1,0:T(8,128)(2,1)S(1)}, u32[]{:S(2)}, u32[]{:S(2)}) collective-permute-start(bf16[15,256]{1,0:T(8,128)(2,1)S(1)} %slice.296), channel_id=1, source_target_pairs={{0,4},{4,8},{8,12},{12,16},{16,20},{20,24},{24,28},{28,32},{32,36}... | collective-permute-start | bytes 23048 | tf_op jit(solution)/shard_map/ppermute | solution.py:29
  714.8 0.6 collective-permute-done.1
  715.4 3.0 convolution_convert_fusion.1
  718.4 0.2 copy.64
  718.6 17.9 %all_to_all.53 = bf16[4,256,1024]{2,1,0:T(8,128)(2,1)S(1)} all-to-all(bf16[4,256,1024]{2,1,0:T(8,128)(2,1)S(1)} %bitcast.96), channel_id=1, replica_groups=mesh['grp'=2,'sp'=32,'tp'=4] {'tp'}, dimensions={0} | all-to-all | bytes 4194304 | tf_op jit(solution)/shard_map/all_to_all | solution.py:55
  736.5 0.4 convert_reduce_fusion.1
  736.9 0.1 multiply_reduce_fusion.1
  737.0 0.6 broadcast_in_dim.85
  737.6 3.3 all-to-all-start.6
  741.0 4.1 all-to-all-done.6
  745.1 0.2 add_convert_fusion.1
  745.3 0.2 copy.48
  745.5 1.5 broadcast_in_dim.86
  747.0 7.2 all-to-all-start.7
  754.2 15.3 %all-to-all-done.7 = bf16[4,256,1024]{1,2,0:T(8,128)(2,1)S(1)} async-done(((bf16[4,256,1024]{1,2,0:T(8,128)(2,1)}), bf16[4,256,1024]{1,2,0:T(8,128)(2,1)S(1)}, u32[]{:S(2)}, u32[]{:S(2)}) %all-to-all-start.7) | async-done | bytes 2097184 | tf_op jit(solution)/shard_map/all_to_all | solution.py:34
  769.6 0.6 fusion.6
  770.1 0.7 fusion.8
  770.9 2.4 fusion.17
  773.3 18.8 %collective-permute-start.2 = (bf16[15,256]{1,0:T(8,128)(2,1)S(1)}, bf16[15,256]{1,0:T(8,128)(2,1)S(1)}, u32[]{:S(2)}, u32[]{:S(2)}) collective-permute-start(bf16[15,256]{1,0:T(8,128)(2,1)S(1)} %slice.315), channel_id=1, source_target_pairs={{0,4},{4,8},{8,12},{12,16},{16,20},{20,24},{24,28},{28,32},{32,36}... | collective-permute-start | bytes 23048 | tf_op jit(solution)/shard_map/ppermute | solution.py:29
  792.1 0.8 collective-permute-done.2
  792.9 3.0 convolution_convert_fusion
  795.9 0.2 copy.63
  796.1 17.9 %all_to_all.54 = bf16[4,256,1024]{2,1,0:T(8,128)(2,1)S(1)} all-to-all(bf16[4,256,1024]{2,1,0:T(8,128)(2,1)S(1)} %bitcast.97), channel_id=1, replica_groups=mesh['grp'=2,'sp'=32,'tp'=4] {'tp'}, dimensions={0} | all-to-all | bytes 4194304 | tf_op jit(solution)/shard_map/all_to_all | solution.py:55
  813.9 0.4 convert_reduce_fusion
  814.3 0.1 multiply_reduce_fusion
  814.5 0.6 broadcast_in_dim.87
  815.1 3.3 all-to-all-start.9
  818.4 4.0 all-to-all-done.9
  822.5 1.0 add_convert_fusion
  (37 shorter events, 0.4 us)
Async XLA Ops:
  2.7 5.3 copy-start.2
  2.7 5.4 copy-start.3
  2.7 20.6 %all-to-all-start = ((bf16[4,256,1024]{1,2,0:T(8,128)(2,1)}), bf16[4,256,1024]{1,2,0:T(8,128)(2,1)S(1)}, u32[]{:S(2)}, u32[]{:S(2)}) async-start(bf16[4,256,1024]{1,2,0:T(8,128)(2,1)} %broadcast_in_dim.81), calls=%async_computation | async-start | bytes 4194304 | tf_op jit(solution)/shard_map/all_to_all | solution.py:34
  30.7 36.1 %copy-start.4 = (f32[3,4096]{1,0:T(4,128)S(1)}, f32[3,4096]{1,0:T(4,128)}, u32[]{:S(2)}) copy-start(f32[3,4096]{1,0:T(4,128)} %param.8) | copy-start | bytes 147460
  30.7 36.3 %copy-start.6 = (f32[3,256]{1,0:T(4,128)S(1)}, f32[3,256]{1,0:T(4,128)}, u32[]{:S(2)}) copy-start(f32[3,256]{1,0:T(4,128)} %param.11) | copy-start | bytes 9220
  30.7 573.9 %all-to-all-start.1 = ((bf16[32,128,1536]{1,2,0:T(8,128)(2,1)}), bf16[32,128,1536]{1,2,0:T(8,128)(2,1)}, u32[]{:S(2)}, u32[]{:S(2)}) async-start(bf16[32,128,1536]{1,2,0:T(8,128)(2,1)} %stack.2), calls=%async_computation.1 | async-start | bytes 25165824 | tf_op jit(solution)/shard_map/all_to_all | solution.py:16
  611.2 6.4 copy-start.1
  614.9 2.7 copy-start
  618.4 15.8 %collective-permute-start = (bf16[15,256]{1,0:T(8,128)(2,1)S(1)}, bf16[15,256]{1,0:T(8,128)(2,1)S(1)}, u32[]{:S(2)}, u32[]{:S(2)}) collective-permute-start(bf16[15,256]{1,0:T(8,128)(2,1)S(1)} %slice.277), channel_id=1, source_target_pairs={{0,4},{4,8},{8,12},{12,16},{16,20},{20,24},{24,28},{28,32},{32,36}... | collective-permute-start | bytes 23048 | tf_op jit(solution)/shard_map/ppermute | solution.py:29
  638.8 3.8 copy-start.5
  638.8 19.1 %all-to-all-start.2 = ((bf16[4,256,1024]{2,1,0:T(8,128)(2,1)}), bf16[4,256,1024]{2,1,0:T(8,128)(2,1)S(1)}, u32[]{:S(2)}, u32[]{:S(2)}) async-start(bf16[4,256,1024]{2,1,0:T(8,128)(2,1)} %bitcast.95), calls=%async_computation.2 | async-start | bytes 4194304 | tf_op jit(solution)/shard_map/all_to_all | solution.py:55
  659.1 7.4 all-to-all-start.3
  669.5 20.9 %all-to-all-start.4 = ((bf16[4,256,1024]{1,2,0:T(8,128)(2,1)}), bf16[4,256,1024]{1,2,0:T(8,128)(2,1)S(1)}, u32[]{:S(2)}, u32[]{:S(2)}) async-start(bf16[4,256,1024]{1,2,0:T(8,128)(2,1)} %broadcast_in_dim.84), calls=%async_computation.4 | async-start | bytes 4194304 | tf_op jit(solution)/shard_map/all_to_all | solution.py:34
  694.1 21.2 %collective-permute-start.1 = (bf16[15,256]{1,0:T(8,128)(2,1)S(1)}, bf16[15,256]{1,0:T(8,128)(2,1)S(1)}, u32[]{:S(2)}, u32[]{:S(2)}) collective-permute-start(bf16[15,256]{1,0:T(8,128)(2,1)S(1)} %slice.296), channel_id=1, source_target_pairs={{0,4},{4,8},{8,12},{12,16},{16,20},{20,24},{24,28},{28,32},{32,36}... | collective-permute-start | bytes 23048 | tf_op jit(solution)/shard_map/ppermute | solution.py:29
  737.6 7.4 all-to-all-start.6
  747.0 22.6 %all-to-all-start.7 = ((bf16[4,256,1024]{1,2,0:T(8,128)(2,1)}), bf16[4,256,1024]{1,2,0:T(8,128)(2,1)S(1)}, u32[]{:S(2)}, u32[]{:S(2)}) async-start(bf16[4,256,1024]{1,2,0:T(8,128)(2,1)} %broadcast_in_dim.86), calls=%async_computation.7 | async-start | bytes 4194304 | tf_op jit(solution)/shard_map/all_to_all | solution.py:34
  773.3 19.6 %collective-permute-start.2 = (bf16[15,256]{1,0:T(8,128)(2,1)S(1)}, bf16[15,256]{1,0:T(8,128)(2,1)S(1)}, u32[]{:S(2)}, u32[]{:S(2)}) collective-permute-start(bf16[15,256]{1,0:T(8,128)(2,1)S(1)} %slice.315), channel_id=1, source_target_pairs={{0,4},{4,8},{8,12},{12,16},{16,20},{20,24},{24,28},{28,32},{32,36}... | collective-permute-start | bytes 23048 | tf_op jit(solution)/shard_map/ppermute | solution.py:29
  815.1 7.4 all-to-all-start.9
